TPU v7x, 32 devices: a whole 2x2x4 slice. The times are simulated.
32 devices in a mesh: sp: 16 (over z, y, x), dp: 2 (over core).
Axes of the slice: x: 2, y: 2, z: 4, core: 2. Of those that a mesh axis runs over, the one named last changes fastest.
Arguments:
- inputs: bfloat16 [2, 2048, 2048], P('dp', 'sp'), may hold values from -6 to 6
- conv_weight: bfloat16 [4, 2048], replicated, may hold values from -3 to 3
- gate_weight: bfloat16 [2, 8, 256, 256], P(None, 'dp'), may hold values from -0.375 to 0.375
- rate_param: float32 [2048], replicated, may hold values from 4 to 12.5
- pace: float32 [2, 2048], P('dp'), may hold values from 0.5 to 30000
Outputs:
- recurrent: bfloat16 [2, 2048, 2048], P('dp', 'sp')
All inputs are finite; a program needn't handle non-finite values.
Results may differ from a plain program's by a relative error of at most 0.008.
Values may be sent and summed in bfloat16 or wider, within the bound.
A program may use at most 128 MiB of HBM per device.

v0:
```python
import jax
import jax.numpy as jnp
from jax import lax
from jax.sharding import PartitionSpec as P

HEADS = 8
BLOCK = 256
CONV = 4
gate_power = 8.0


def passed_along(array, axis, by):
    devices = lax.axis_size(axis)
    pairs = [(i, i + by) for i in range(devices) if 0 <= i + by < devices]
    return lax.ppermute(array, axis, pairs)


def combine(earlier, later):
    decay_e, state_e = earlier
    decay_l, state_l = later
    return (decay_e * decay_l, decay_l * state_e + state_l)


def lru_terms(pre_recur, pre_input, values, rate_col, pace_col):
    recur_gate = jax.nn.sigmoid(pre_recur.astype(jnp.float32))
    input_gate = jax.nn.sigmoid(pre_input.astype(jnp.float32))
    log_decay = -gate_power * pace_col * recur_gate * jax.nn.softplus(-rate_col)
    decay = jnp.exp(log_decay)
    drive = jnp.sqrt(-jnp.expm1(2.0 * log_decay)) * input_gate * values.astype(jnp.float32)
    return (decay, drive)


def body(inputs, conv_weight, gate_weight, rate_param, pace):
    own_rows = inputs[0].T
    width = own_rows.shape[0]
    count = own_rows.shape[1]
    earlier = passed_along(own_rows[:, count - (CONV - 1) :], "sp", 1)
    padded = jnp.concatenate([earlier, own_rows], axis=1).astype(jnp.float32)
    conv_taps = conv_weight.astype(jnp.float32)
    conv_out = jnp.zeros((width, count), jnp.float32)
    for tap in range(CONV):
        conv_out = conv_out + conv_taps[tap][:, None] * padded[:, tap : tap + count]
    conv_out = conv_out.astype(jnp.bfloat16)
    by_head = conv_out.reshape(HEADS, BLOCK, count)
    preact = (
        jnp.einsum(
            "hit,ghij->ghjt",
            by_head,
            lax.all_gather(gate_weight, "dp", axis=1, tiled=True),
            preferred_element_type=jnp.float32,
        )
        .astype(jnp.bfloat16)
        .reshape(2, width, count)
    )
    stacked = jnp.stack([conv_out, preact[0], preact[1]])
    arrived = lax.all_to_all(stacked, "sp", split_axis=1, concat_axis=2, tiled=True)
    lanes = arrived.shape[1]
    lane_rates = lax.dynamic_slice_in_dim(rate_param, lax.axis_index("sp") * lanes, lanes)
    decay, drive = lru_terms(
        arrived[1], arrived[2], arrived[0], lane_rates[:, None], pace[0][None, :]
    )
    _, state = lax.associative_scan(combine, (decay, drive), axis=1)
    result = lax.all_to_all(
        state.astype(jnp.bfloat16), "sp", split_axis=1, concat_axis=0, tiled=True
    )
    return result.T[None]


def solution(mesh):
    return jax.shard_map(
        body,
        mesh=mesh,
        in_specs=(P("dp", "sp", None), P(), P(None, "dp", None, None), P(), P("dp", None)),
        out_specs=P("dp", "sp", None),
        check_vma=False,
    )
```

profile of v0, /device:TPU:0, one launch (start us, length us, event | category | flops | bytes accessed | tf_op | source)
XLA Modules:
  0.0 151.2 jit_solution(12866272480589293699)
XLA Ops:
  6.5 2.3 %copy.31 = bf16[2,4,256,256]{3,2,0,1:T(8,128)(2,1)} copy(bf16[2,4,256,256]{3,2,1,0:T(8,128)(2,1)} %param.7) | data formatting | bytes 2097152 | tf_op args[2]
  9.4 4.9 %collective-permute-start = (bf16[2048,3]{1,0:T(8,128)(2,1)S(1)}, bf16[2048,3]{1,0:T(8,128)(2,1)S(1)}, u32[]{:S(2)}, u32[]{:S(2)}) collective-permute-start(bf16[2048,3]{1,0:T(8,128)(2,1)S(1)} %slice.406), channel_id=1, source_target_pairs={{0,2},{2,4},{4,6},{6,8},{8,10},{10,12},{12,14},{14,16},{16,18},{18... | collective-permute-start | bytes 36872 | tf_op jit(solution)/shard_map/ppermute | solution.py:15
  14.4 11.1 %collective-permute-done = bf16[2048,3]{1,0:T(8,128)(2,1)S(1)} collective-permute-done((bf16[2048,3]{1,0:T(8,128)(2,1)S(1)}, bf16[2048,3]{1,0:T(8,128)(2,1)S(1)}, u32[]{:S(2)}, u32[]{:S(2)}) %collective-permute-start) | collective-permute-done | bytes 12320 | tf_op jit(solution)/shard_map/ppermute | solution.py:15
  25.4 0.4 maximum_convert_fusion
  25.9 2.2 %fusion.29 = bf16[1,2048,128]{2,1,0:T(8,128)(2,1)S(1)} fusion(f32[2048,131]{1,0:T(8,128)S(1)} %maximum_convert_fusion, f32[2048]{0:T(1024)S(1)} %bitcast.61, f32[2048]{0:T(1024)S(1)} %bitcast.59, f32[2048]{0:T(1024)S(1)} %bitcast.57, f32[2048]{0:T(1024)S(1)} %bitcast.55), kind=kLoop, calls=%fused_computation.75 | loop fusion | flops 2097152 | bytes 4751360 | tf_op jit(solution)/shard_map/stack | solution.py:55
  28.0 2.2 %fusion.2 = bf16[2048,128]{1,0:T(8,128)(2,1)S(1)} fusion(f32[2048,131]{1,0:T(8,128)S(1)} %maximum_convert_fusion, f32[2048]{0:T(1024)S(1)} %bitcast.62, f32[2048]{0:T(1024)S(1)} %bitcast.60, f32[2048]{0:T(1024)S(1)} %bitcast.58, f32[2048]{0:T(1024)S(1)} %bitcast.56), kind=kLoop, calls=%fused_computation.5 | loop fusion | flops 2097152 | bytes 4751360 | tf_op jit(solution)/shard_map/convert_element_type | solution.py:43
  30.2 2.1 %fusion = bf16[2,8,256,128]{2,3,0,1:T(8,128)(2,1)S(1)} fusion(bf16[8,256,128,1]{2,1,3,0:T(8,128)(2,1)S(1)} %bitcast.49, bf16[2,8,256,256]{3,2,0,1:T(8,128)(2,1)} %all-gather.2.cloned.1.call-done), kind=kOutput, calls=%fused_computation.2 | convolution fusion | flops 268959744 | bytes 3670016 | tf_op jit(solution)/shard_map/hit,ghij->ghjt/dot_general | solution.py:46
  33.1 10.7 %copy.35 = bf16[3,2048,128]{2,0,1:T(4,128)(2,1)} copy(bf16[3,2048,128]{2,1,0:T(8,128)(2,1)S(1)} %pad_maximum_fusion) | data formatting | bytes 3145728 | tf_op jit(solution)/shard_map/stack | solution.py:55
  43.9 8.0 %all-to-all-start = ((bf16[3,2048,128]{2,0,1:T(4,128)(2,1)}), bf16[3,2048,128]{2,0,1:T(4,128)(2,1)S(1)}, u32[]{:S(2)}, u32[]{:S(2)}) async-start(bf16[3,2048,128]{2,0,1:T(4,128)(2,1)} %copy.35), calls=%async_computation | async-start | bytes 4194304 | tf_op jit(solution)/shard_map/all_to_all | solution.py:56
  51.9 0.8 compare_select_fusion
  52.7 41.6 %all-to-all-done = bf16[3,2048,128]{2,0,1:T(4,128)(2,1)S(1)} async-done(((bf16[3,2048,128]{2,0,1:T(4,128)(2,1)}), bf16[3,2048,128]{2,0,1:T(4,128)(2,1)S(1)}, u32[]{:S(2)}, u32[]{:S(2)}) %all-to-all-start) | async-done | bytes 1572896 | tf_op jit(solution)/shard_map/all_to_all | solution.py:56
  94.6 0.6 add_divide_fusion.1
  95.2 1.3 copy.39
  96.5 1.4 copy.37
  97.8 1.3 copy.38
  99.2 2.4 %fusion.6 = (f32[128,2048]{0,1:T(8,128)S(1)}, f32[128,2048]{0,1:T(8,128)S(1)}) fusion(f32[1,128,16,128]{1,3,2,0:T(8,128)} %copy.37, f32[128]{0:T(128)S(1)} %compare_select_fusion, f32[2048]{0:T(1024)S(1)} %bitcast.63, f32[1,128,16,128]{1,3,2,0:T(8,128)S(1)} %copy-done, f32[1,128,16,128]{1,3,2,0:T(8,128)} %copy.38), kind=kLoop, calls=%fused_computation.19 | loop fusion | flops 1572864 | bytes 5251584 | tf_op jit(solution)/shard_map/exp | solution.py:28
  101.6 0.7 slice.328
  102.3 2.1 %slice.324 = f32[128,1024]{0,1:T(8,128)} slice(f32[128,2048]{0,1:T(8,128)S(1)} %get-tuple-element.7), slice={[0:128:1], [1:2048:2]} | slice | bytes 1048576 | tf_op jit(solution)/shard_map/slice | solution.py:62
  104.4 0.7 slice.323
  105.1 0.7 slice.404
  105.8 2.0 %slice.326 = f32[128,1024]{0,1:T(8,128)} slice(f32[128,2048]{0,1:T(8,128)S(1)} %get-tuple-element.8), slice={[0:128:1], [1:2048:2]} | slice | bytes 1048576 | tf_op jit(solution)/shard_map/slice | solution.py:62
  107.8 2.0 %slice.325 = f32[128,1024]{0,1:T(8,128)} slice(f32[128,2048]{0,1:T(8,128)S(1)} %get-tuple-element.8), slice={[0:128:1], [0:2047:2]} | slice | bytes 1048576 | tf_op jit(solution)/shard_map/slice | solution.py:62
  109.9 1.3 fusion.15
  111.2 0.4 slice.334
  111.6 0.4 slice.330
  112.0 0.4 slice.329
  112.4 0.4 slice.402
  112.8 0.4 slice.332
  113.2 1.4 slice.331
  114.6 1.0 fusion.16
  119.0 24.0 %all_to_all.34 = bf16[128,16,128]{0,2,1:T(8,128)(2,1)S(1)} all-to-all(bf16[128,16,128]{0,2,1:T(8,128)(2,1)S(1)} %bitcast.50), channel_id=1, replica_groups=mesh['sp'=16,'dp'=2] {'sp'}, dimensions={1} | all-to-all | bytes 1048576 | tf_op jit(solution)/shard_map/all_to_all | solution.py:63
  143.3 1.0 copy.41
  (139 shorter events, 4.8 us)
Async XLA Ops:
  6.5 2.4 %copy-start.2 = (bf16[1,128,2048]{2,1,0:T(8,128)(2,1)S(1)}, bf16[1,128,2048]{2,1,0:T(8,128)(2,1)}, u32[]{:S(2)}) copy-start(bf16[1,128,2048]{2,1,0:T(8,128)(2,1)} %param.5) | copy-start | bytes 1572868
  6.5 23.7 %all-gather.2.cloned.1.call-start = ((), (), s32[]{:S(2)}) async-start(), calls=%async_computation.2 | async-start | bytes 3145728 | tf_op jit(solution)/shard_map/all_gather | solution.py:49
  8.9 5.4 %copy-start.3 = (bf16[4,2048]{1,0:T(4,128)(2,1)S(1)}, bf16[4,2048]{1,0:T(4,128)(2,1)}, u32[]{:S(2)}) copy-start(bf16[4,2048]{1,0:T(4,128)(2,1)} %param.6) | copy-start | bytes 49156
  9.4 16.0 %collective-permute-start = (bf16[2048,3]{1,0:T(8,128)(2,1)S(1)}, bf16[2048,3]{1,0:T(8,128)(2,1)S(1)}, u32[]{:S(2)}, u32[]{:S(2)}) collective-permute-start(bf16[2048,3]{1,0:T(8,128)(2,1)S(1)} %slice.406), channel_id=1, source_target_pairs={{0,2},{2,4},{4,6},{6,8},{8,10},{10,12},{12,14},{14,16},{16,18},{18... | collective-permute-start | bytes 36872 | tf_op jit(solution)/shard_map/ppermute | solution.py:15
  43.9 8.8 %copy-start.4 = (f32[1,2048]{1,0:T(1,128)S(1)}, f32[1,2048]{1,0:T(1,128)}, u32[]{:S(2)}) copy-start(f32[1,2048]{1,0:T(1,128)} %param.9) | copy-start | bytes 24580
  43.9 50.4 %all-to-all-start = ((bf16[3,2048,128]{2,0,1:T(4,128)(2,1)}), bf16[3,2048,128]{2,0,1:T(4,128)(2,1)S(1)}, u32[]{:S(2)}, u32[]{:S(2)}) async-start(bf16[3,2048,128]{2,0,1:T(4,128)(2,1)} %copy.35), calls=%async_computation | async-start | bytes 4194304 | tf_op jit(solution)/shard_map/all_to_all | solution.py:56
  96.5 2.7 %copy-start = (f32[1,128,16,128]{1,3,2,0:T(8,128)S(1)}, f32[1,128,16,128]{1,3,2,0:T(8,128)}, u32[]{:S(2)}) copy-start(f32[1,128,16,128]{1,3,2,0:T(8,128)} %copy.39) | copy-start | bytes 3145732
  105.1 4.8 %copy-start.1 = (f32[128,1024]{0,1:T(8,128)S(1)}, f32[128,1024]{0,1:T(8,128)}, u32[]{:S(2)}) copy-start(f32[128,1024]{0,1:T(8,128)} %slice.324) | copy-start | bytes 1572868
Sparse Core Ops, SparseCore 0:
  9.0 13.2 all-gather.1
where the time goes:
time: 152 us; the launch traced here: 151 us
  waiting for transfers between devices  52.7 us (35%)
  local copies, waits for them, and re-layouts  33.3 us (22%)
  blocking collectives  24 us (16%)
  between operations  14.2 us (9%)
  starting transfers between devices  12.9 us (8%)
  other arithmetic  11.8 us (8%)
  matrix products  2.09 us (1%)
    all_to_all x1, waiting for transfers between devices, body(): lax.all_to_all(stacked, 'sp', split_axis=1, concat_axis=2, tiled=True)  41.6 us
    all_to_all x1, blocking collectives, body(): lax.all_to_all(state.astype(jnp.bfloat16), 'sp', split_axis=1, concat_axi...  24 us
    slice x67, local copies, waits for them, and re-layouts, body(): _, state = lax.associative_scan(combine, (decay, drive), axis=1)  13.2 us
    ppermute x1, waiting for transfers between devices, passed_along(): return lax.ppermute(array, axis, pairs)  11.1 us
    another operation x1, local copies, waits for them, and re-layouts, body(): stacked = jnp.stack([conv_out, preact[0], preact[1]])  10.7 us
    all_to_all x1, starting transfers between devices, body(): lax.all_to_all(stacked, 'sp', split_axis=1, concat_axis=2, tiled=True)  8 us
    ppermute x1, starting transfers between devices, passed_along(): return lax.ppermute(array, axis, pairs)  4.9 us
  transfers between devices with their start and end apart: 3, of which 2 were waited for; matrix products, arithmetic and copies ran while one was open for 4% of the time, Pallas kernels for 0%

commit v1 on v0

--- a/solution.py
+++ b/solution.py
@@ -53,7 +53,10 @@
         .reshape(2, width, count)
     )
     stacked = jnp.stack([conv_out, preact[0], preact[1]])
-    arrived = lax.all_to_all(stacked, "sp", split_axis=1, concat_axis=2, tiled=True)
+    arrived = jnp.concatenate(
+        lax.all_to_all(jnp.stack(jnp.split(stacked, lax.axis_size("sp"), axis=1)), "sp", 0, 0),
+        axis=2,
+    )
     lanes = arrived.shape[1]
     lane_rates = lax.dynamic_slice_in_dim(rate_param, lax.axis_index("sp") * lanes, lanes)
     decay, drive = lru_terms(

time: 152 us -> 143 us (0.941)
  waiting for transfers between devices: 52.7 us -> 43.8 us
  blocking collectives: 24 us -> 21.6 us
  other arithmetic: 11.8 us -> 14.1 us
    another operation x1, local copies, waits for them, and re-layouts: 10.7 us -> 0.65 us  [body(): jnp.stack(jnp.split(stacked, lax.axis_size('sp'), axis=1))]
    unnamed x12 -> x27, local copies, waits for them, and re-layouts: 2.62 us -> 12.3 us
    all_to_all x1, waiting for transfers between devices: 41.6 us -> 32.7 us  [body(): lax.all_to_all(jnp.stack(jnp.split(stacked, lax.axis_size('sp'), axis=1))...]
    all_to_all x1, blocking collectives: 24 us -> 21.6 us  [body(): lax.all_to_all(state.astype(jnp.bfloat16), 'sp', split_axis=1, concat_axi...]
where the time goes in v1:
time: 143 us
  waiting for transfers between devices  43.8 us (31%)
  local copies, waits for them, and re-layouts  34 us (24%)
  blocking collectives  21.6 us (15%)
  between operations  14.2 us (10%)
  other arithmetic  14.1 us (10%)
  starting transfers between devices  12.9 us (9%)
  matrix products  2.09 us (1%)
    all_to_all x1, waiting for transfers between devices, body(): lax.all_to_all(jnp.stack(jnp.split(stacked, lax.axis_size('sp'), axis=1))...  32.7 us
    all_to_all x1, blocking collectives, body(): lax.all_to_all(state.astype(jnp.bfloat16), 'sp', split_axis=1, concat_axi...  21.6 us
    slice x67, local copies, waits for them, and re-layouts, body(): _, state = lax.associative_scan(combine, (decay, drive), axis=1)  13.2 us
    unnamed x27, local copies, waits for them, and re-layouts  12.3 us
    ppermute x1, waiting for transfers between devices, passed_along(): return lax.ppermute(array, axis, pairs)  11.1 us
    all_to_all x1, starting transfers between devices, body(): lax.all_to_all(jnp.stack(jnp.split(stacked, lax.axis_size('sp'), axis=1))...  7.98 us
    ppermute x1, starting transfers between devices, passed_along(): return lax.ppermute(array, axis, pairs)  4.9 us
  transfers between devices with their start and end apart: 3, of which 2 were waited for; matrix products, arithmetic and copies ran while one was open for 4% of the time, Pallas kernels for 0%

profile of v1, /device:TPU:0, one launch (start us, length us, event | category | flops | bytes accessed | tf_op | source)
XLA Modules:
  0.0 142.7 jit_solution(10216234845656799369)
XLA Ops:
  6.5 2.3 %copy.24 = bf16[2,4,256,256]{3,2,0,1:T(8,128)(2,1)} copy(bf16[2,4,256,256]{3,2,1,0:T(8,128)(2,1)} %param.7) | data formatting | bytes 2097152 | tf_op args[2]
  9.4 4.9 %collective-permute-start = (bf16[2048,3]{1,0:T(8,128)(2,1)S(1)}, bf16[2048,3]{1,0:T(8,128)(2,1)S(1)}, u32[]{:S(2)}, u32[]{:S(2)}) collective-permute-start(bf16[2048,3]{1,0:T(8,128)(2,1)S(1)} %slice.406), channel_id=1, source_target_pairs={{0,2},{2,4},{4,6},{6,8},{8,10},{10,12},{12,14},{14,16},{16,18},{18... | collective-permute-start | bytes 36872 | tf_op jit(solution)/shard_map/ppermute | solution.py:15
  14.4 11.1 %collective-permute-done = bf16[2048,3]{1,0:T(8,128)(2,1)S(1)} collective-permute-done((bf16[2048,3]{1,0:T(8,128)(2,1)S(1)}, bf16[2048,3]{1,0:T(8,128)(2,1)S(1)}, u32[]{:S(2)}, u32[]{:S(2)}) %collective-permute-start) | collective-permute-done | bytes 12320 | tf_op jit(solution)/shard_map/ppermute | solution.py:15
  25.9 2.2 %fusion.45 = bf16[1,2048,128]{2,1,0:T(8,128)(2,1)S(1)} fusion(f32[2048,131]{1,0:T(8,128)S(1)} %maximum_convert_fusion, f32[2048]{0:T(1024)S(1)} %bitcast.123, f32[2048]{0:T(1024)S(1)} %bitcast.121, f32[2048]{0:T(1024)S(1)} %bitcast.119, f32[2048]{0:T(1024)S(1)} %bitcast.117), kind=kLoop, calls=%fused_computation.107 | loop fusion | flops 2097152 | bytes 4751360 | tf_op jit(solution)/shard_map/stack | solution.py:55
  28.0 2.2 %fusion.2 = bf16[2048,128]{1,0:T(8,128)(2,1)S(1)} fusion(f32[2048,131]{1,0:T(8,128)S(1)} %maximum_convert_fusion, f32[2048]{0:T(1024)S(1)} %bitcast.124, f32[2048]{0:T(1024)S(1)} %bitcast.122, f32[2048]{0:T(1024)S(1)} %bitcast.120, f32[2048]{0:T(1024)S(1)} %bitcast.118), kind=kLoop, calls=%fused_computation.5 | loop fusion | flops 2097152 | bytes 4751360 | tf_op jit(solution)/shard_map/convert_element_type | solution.py:43
  30.2 2.1 %fusion = bf16[2,8,256,128]{2,3,0,1:T(8,128)(2,1)S(1)} fusion(bf16[8,256,128,1]{2,1,3,0:T(8,128)(2,1)S(1)} %bitcast.111, bf16[2,8,256,256]{3,2,0,1:T(8,128)(2,1)} %all-gather.2.cloned.1.call-done), kind=kOutput, calls=%fused_computation.2 | convolution fusion | flops 268959744 | bytes 3670016 | tf_op jit(solution)/shard_map/hit,ghij->ghjt/dot_general | solution.py:46
  35.7 0.7 fusion.21
  36.4 0.7 fusion.20
  37.0 0.7 fusion.19
  38.3 0.7 fusion.17
  39.0 0.7 fusion.16
  41.5 0.7 fusion.12
  43.5 8.0 %all-to-all-start = ((bf16[16,3,128,128]{3,2,1,0:T(8,128)(2,1)}), bf16[16,3,128,128]{3,2,1,0:T(8,128)(2,1)S(1)}, u32[]{:S(2)}, u32[]{:S(2)}) async-start(bf16[16,3,128,128]{3,2,1,0:T(8,128)(2,1)} %fusion.10), calls=%async_computation | async-start | bytes 3145728 | tf_op jit(solution)/shard_map/all_to_all | solution.py:57
  51.5 0.8 compare_select_fusion
  52.3 32.7 %all-to-all-done = bf16[16,3,128,128]{3,2,1,0:T(8,128)(2,1)S(1)} async-done(((bf16[16,3,128,128]{3,2,1,0:T(8,128)(2,1)}), bf16[16,3,128,128]{3,2,1,0:T(8,128)(2,1)S(1)}, u32[]{:S(2)}, u32[]{:S(2)}) %all-to-all-start) | async-done | bytes 1572896 | tf_op jit(solution)/shard_map/all_to_all | solution.py:57
  85.0 1.1 slice_convert_fusion
  86.0 1.5 %add_divide_fusion.1 = (f32[1,128,16,128]{3,1,0,2:T(8,128)}, f32[1,128,16,128]{3,1,0,2:T(8,128)S(1)}) fusion(bf16[3,128,16,128]{3,1,0,2:T(8,128)(2,1)S(1)} %bitcast.108), kind=kLoop, calls=%fused_computation.18 | loop fusion | flops 2097152 | bytes 3145728 | tf_op jit(solution)/shard_map/div | solution.py:25
  87.6 2.7 %copy.30 = f32[1,128,16,128]{1,3,2,0:T(8,128)} copy(f32[1,128,16,128]{3,1,0,2:T(8,128)} %slice_convert_fusion) | data formatting | bytes 2097152 | tf_op jit(solution)/shard_map/convert_element_type | solution.py:29
  90.2 1.3 copy.28
  91.5 1.3 copy.29
  92.8 2.7 %fusion.6 = (f32[128,2048]{0,1:T(8,128)S(1)}, f32[128,2048]{0,1:T(8,128)S(1)}) fusion(f32[1,128,16,128]{1,3,2,0:T(8,128)} %copy.28, f32[128]{0:T(128)S(1)} %compare_select_fusion, f32[2048]{0:T(1024)S(1)} %bitcast.125, f32[1,128,16,128]{1,3,2,0:T(8,128)} %copy.30, f32[1,128,16,128]{1,3,2,0:T(8,128)} %copy.29), kind=kLoop, calls=%fused_computation.19 | loop fusion | flops 1572864 | bytes 5251584 | tf_op jit(solution)/shard_map/exp | solution.py:28
  95.6 0.7 slice.328
  96.3 2.1 %slice.324 = f32[128,1024]{0,1:T(8,128)} slice(f32[128,2048]{0,1:T(8,128)S(1)} %get-tuple-element.7), slice={[0:128:1], [1:2048:2]} | slice | bytes 1048576 | tf_op jit(solution)/shard_map/slice | solution.py:65
  98.3 0.7 slice.323
  99.0 0.7 slice.404
  99.8 2.0 %slice.326 = f32[128,1024]{0,1:T(8,128)} slice(f32[128,2048]{0,1:T(8,128)S(1)} %get-tuple-element.8), slice={[0:128:1], [1:2048:2]} | slice | bytes 1048576 | tf_op jit(solution)/shard_map/slice | solution.py:65
  101.8 2.0 %slice.325 = f32[128,1024]{0,1:T(8,128)} slice(f32[128,2048]{0,1:T(8,128)S(1)} %get-tuple-element.8), slice={[0:128:1], [0:2047:2]} | slice | bytes 1048576 | tf_op jit(solution)/shard_map/slice | solution.py:65
  103.9 1.3 fusion.31
  107.2 1.4 slice.331
  108.6 1.0 fusion.32
  113.0 21.6 %all_to_all.24 = bf16[128,16,128]{0,2,1:T(8,128)(2,1)S(1)} all-to-all(bf16[128,16,128]{0,2,1:T(8,128)(2,1)S(1)} %bitcast.112), channel_id=1, replica_groups=mesh['sp'=16,'dp'=2] {'sp'}, dimensions={1} | all-to-all | bytes 1048576 | tf_op jit(solution)/shard_map/all_to_all | solution.py:66
  134.9 1.0 copy.32
  (153 shorter events, 13.3 us)
Async XLA Ops:
  6.5 2.4 %copy-start.2 = (bf16[1,128,2048]{2,1,0:T(8,128)(2,1)S(1)}, bf16[1,128,2048]{2,1,0:T(8,128)(2,1)}, u32[]{:S(2)}) copy-start(bf16[1,128,2048]{2,1,0:T(8,128)(2,1)} %param.5) | copy-start | bytes 1572868
  6.5 23.7 %all-gather.2.cloned.1.call-start = ((), (), s32[]{:S(2)}) async-start(), calls=%async_computation.2 | async-start | bytes 3145728 | tf_op jit(solution)/shard_map/all_gather | solution.py:49
  8.9 5.4 %copy-start.3 = (bf16[4,2048]{1,0:T(4,128)(2,1)S(1)}, bf16[4,2048]{1,0:T(4,128)(2,1)}, u32[]{:S(2)}) copy-start(bf16[4,2048]{1,0:T(4,128)(2,1)} %param.6) | copy-start | bytes 49156
  9.4 16.0 %collective-permute-start = (bf16[2048,3]{1,0:T(8,128)(2,1)S(1)}, bf16[2048,3]{1,0:T(8,128)(2,1)S(1)}, u32[]{:S(2)}, u32[]{:S(2)}) collective-permute-start(bf16[2048,3]{1,0:T(8,128)(2,1)S(1)} %slice.406), channel_id=1, source_target_pairs={{0,2},{2,4},{4,6},{6,8},{8,10},{10,12},{12,14},{14,16},{16,18},{18... | collective-permute-start | bytes 36872 | tf_op jit(solution)/shard_map/ppermute | solution.py:15
  43.5 8.8 %copy-start.4 = (f32[1,2048]{1,0:T(1,128)S(1)}, f32[1,2048]{1,0:T(1,128)}, u32[]{:S(2)}) copy-start(f32[1,2048]{1,0:T(1,128)} %param.9) | copy-start | bytes 24580
  43.5 41.5 %all-to-all-start = ((bf16[16,3,128,128]{3,2,1,0:T(8,128)(2,1)}), bf16[16,3,128,128]{3,2,1,0:T(8,128)(2,1)S(1)}, u32[]{:S(2)}, u32[]{:S(2)}) async-start(bf16[16,3,128,128]{3,2,1,0:T(8,128)(2,1)} %fusion.10), calls=%async_computation | async-start | bytes 3145728 | tf_op jit(solution)/shard_map/all_to_all | solution.py:57
  87.6 2.7 %copy-start = (f32[1,128,16,128]{3,1,0,2:T(8,128)S(1)}, f32[1,128,16,128]{3,1,0,2:T(8,128)}, u32[]{:S(2)}) copy-start(f32[1,128,16,128]{3,1,0,2:T(8,128)} %get-tuple-element.5) | copy-start | bytes 3145732
  99.0 4.8 %copy-start.1 = (f32[128,1024]{0,1:T(8,128)S(1)}, f32[128,1024]{0,1:T(8,128)}, u32[]{:S(2)}) copy-start(f32[128,1024]{0,1:T(8,128)} %slice.324) | copy-start | bytes 1572868
Sparse Core Ops, SparseCore 0:
  9.0 13.2 all-gather.1
